TPU v7x, 32 devices: a whole 2x2x4 slice. The times are simulated.
32 devices in a mesh: grp: 2 (over y), fs: 4 (over z), tp: 4 (over x, core).
Axes of the slice: x: 2, y: 2, z: 4, core: 2. Of those that a mesh axis runs over, the one named last changes fastest.
Arguments:
- tokens: bfloat16 [4096, 2048], P(('grp', 'fs')), parts along dimension 0, may hold values from -6 to 6
- pre_gain: float32 [2048], replicated, may hold values from 0.1 to 1.9
- gate_weight: float32 [2048, 5632], P('fs', 'tp'), may hold values from -0.125 to 0.125
- gate_scale: float32 [5632], P('tp'), may hold values from 0.5 to 2
- up_weight: float32 [2048, 5632], P('fs', 'tp'), may hold values from -0.125 to 0.125
- up_scale: float32 [5632], P('tp'), may hold values from 0.5 to 2
- down_weight: float32 [5632, 2048], P('tp', 'fs'), may hold values from -0.078125 to 0.078125
- down_scale: float32 [2048], replicated, may hold values from 0.3 to 3
- post_gain: float32 [2048], replicated, may hold values from 0.1 to 1.9
Outputs:
- mixed: bfloat16 [4096, 2048], P(('grp', 'fs')), parts along dimension 0
There are 2 independent parts, one for each index of `grp`. A program takes and returns all parts, laid end to end along the dimension named above; an argument that names none is the same for every part. Nothing has to cross between parts.
All inputs are finite; a program needn't handle non-finite values.
Results may differ from a plain program's by a relative error of at most 0.018.
Values may be sent and summed in bfloat16 or wider, within the bound.
A program may use at most 64 MiB of HBM per device.

v0:
```python
import jax
import jax.numpy as jnp
from jax import lax
from jax.sharding import PartitionSpec as P

EPS = 1e-06


def finish(summed, down_scale, post_gain):
    branch = summed * down_scale
    return (
        branch * lax.rsqrt(jnp.mean(branch * branch, axis=-1, keepdims=True) + EPS) * post_gain
    ).astype(jnp.bfloat16)


def body(
    tokens,
    pre_gain,
    gate_weight,
    gate_scale,
    up_weight,
    up_scale,
    down_weight,
    down_scale,
    post_gain,
):
    rows = tokens.astype(jnp.float32)
    normed = (
        rows * lax.rsqrt(jnp.mean(rows * rows, axis=-1, keepdims=True) + EPS) * pre_gain
    ).astype(jnp.bfloat16)
    gate_low = gate_weight.astype(jnp.bfloat16)
    up_low = up_weight.astype(jnp.bfloat16)
    down_low = down_weight.astype(jnp.bfloat16)
    gate_full, up_full = (
        lax.all_gather(gate_low, "fs", axis=0, tiled=True),
        lax.all_gather(up_low, "fs", axis=0, tiled=True),
    )
    gate = jnp.dot(normed, gate_full, preferred_element_type=jnp.float32) * gate_scale
    up = jnp.dot(normed, up_full, preferred_element_type=jnp.float32) * up_scale
    hidden = (jax.nn.silu(gate) * up).astype(jnp.bfloat16)
    down_full = lax.all_gather(down_low, "fs", axis=1, tiled=True)
    partial_value = jnp.dot(hidden, down_full, preferred_element_type=jnp.float32)
    summed = lax.psum(partial_value.astype(jnp.bfloat16), "tp").astype(jnp.float32)
    return finish(summed, down_scale, post_gain)


def solution(mesh):
    in_specs = (
        P(("grp", "fs"), None),
        P(),
        P("fs", "tp"),
        P("tp"),
        P("fs", "tp"),
        P("tp"),
        P("tp", "fs"),
        P(),
        P(),
    )
    out_specs = P(("grp", "fs"), None)
    return jax.shard_map(body, mesh=mesh, in_specs=in_specs, out_specs=out_specs, check_vma=False)
```

profile of v0, /device:TPU:0, one launch (start us, length us, event | category | flops | bytes accessed | tf_op | source)
XLA Modules:
  0.0 406.5 jit_solution(4546783857032367066)
XLA Ops:
  6.5 0.0 all-gather.4.cloned.1.call-start
  6.5 3.2 convert_element_type.29
  9.8 0.0 all-gather.4.cloned.1.call-update
  9.8 0.0 all-gather.6.cloned.1.call-start
  9.9 0.0 copy-done.1
  9.9 1.3 convert_element_type.30
  11.1 0.0 all-gather.6.cloned.1.call-update
  11.2 0.0 copy-start.2
  11.2 0.0 copy-start.5
  11.2 0.0 copy-start.6
  11.2 0.0 all-gather.8.cloned.1.call-start
  11.2 3.2 convert_element_type.32
  14.5 0.0 all-gather.8.cloned.1.call-update
  14.5 0.0 all-reduce.2.cloned.1.call-start
  14.5 0.0 copy-done.2
  14.6 0.5 fusion
  15.0 0.0 copy-start.7
  15.1 104.3 %all-gather.4.cloned.1.call-done = bf16[2048,1408]{1,0:T(8,128)(2,1)} async-done(((bf16[512,1408]{1,0:T(8,128)(2,1)}), bf16[2048,1408]{1,0:T(8,128)(2,1)}) %all-gather.4.cloned.1.call-update) | async-done | bytes 5767184 | tf_op jit(solution)/shard_map/all_gather | solution.py:35
  119.4 0.0 copy-done.5
  119.4 0.0 copy-done.6
  119.4 7.6 %convolution_multiply_fusion.1 = f32[512,1408]{1,0:T(8,128)} fusion(bf16[2048,1408]{1,0:T(8,128)(2,1)} %all-gather.4.cloned.1.call-done, f32[1408]{0:T(1024)S(1)} %copy-done.5, bf16[512,2048]{1,0:T(8,128)(2,1)S(1)} %copy-done.2, f32[2048]{0:T(1024)S(1)} %copy-done.6, f32[512]{0:T(512)S(1)} %add_rsqrt_fusion.1), kind=kOutput, calls=%fused_computation.10 | convolution fusion | flops 2957705216 | bytes 10763776 | tf_op jit(solution)/shard_map/dot_general | solution.py:38
  127.0 98.9 %all-gather.6.cloned.1.call-done = bf16[2048,1408]{1,0:T(8,128)(2,1)} async-done(((bf16[512,1408]{1,0:T(8,128)(2,1)}), bf16[2048,1408]{1,0:T(8,128)(2,1)}) %all-gather.6.cloned.1.call-update) | async-done | bytes 5767184 | tf_op jit(solution)/shard_map/all_gather | solution.py:36
  225.9 106.5 %all-gather.8.cloned.1.call-done = bf16[1408,2048]{1,0:T(8,128)(2,1)} async-done(((bf16[1408,512]{1,0:T(8,128)(2,1)}), bf16[1408,2048]{1,0:T(8,128)(2,1)}) %all-gather.8.cloned.1.call-update) | async-done | bytes 5767184 | tf_op jit(solution)/shard_map/all_gather | solution.py:41
  332.5 0.0 copy-done.7
  332.5 13.3 %convolution_convert_fusion = bf16[512,2048]{1,0:T(8,128)(2,1)} fusion(bf16[1408,2048]{1,0:T(8,128)(2,1)} %all-gather.8.cloned.1.call-done, bf16[2048,1408]{1,0:T(8,128)(2,1)} %all-gather.6.cloned.1.call-done, f32[512,1408]{1,0:T(8,128)} %convolution_multiply_fusion.1, f32[1408]{0:T(1024)S(1)} %copy-done.7, bf16[512,2048]{1,0:T(8,128)(2,1)S(1)} %copy-done.2, ...), kind=kOutput, calls=%fused_computation.12 | convolution fusion | flops 5915869184 | bytes 18628096 | tf_op jit(solution)/shard_map/dot_general | solution.py:42
  345.8 0.0 all-reduce.2.cloned.1.call-update
  345.8 49.8 %all-reduce.2.cloned.1.call-done = bf16[512,2048]{1,0:T(8,128)(2,1)} async-done(((bf16[512,2048]{1,0:T(8,128)(2,1)}), bf16[512,2048]{1,0:T(8,128)(2,1)}) %all-reduce.2.cloned.1.call-update) | async-done | bytes 2097168 | tf_op jit(solution)/shard_map/psum | solution.py:43
  395.6 0.0 copy-done.3
  395.6 2.4 multiply_reduce_fusion
  398.0 0.0 copy-done.4
  398.0 0.0 copy-done
  398.0 2.0 multiply_convert_fusion
  (6 shorter events, 0.0 us)
Async XLA Ops:
  6.5 3.3 copy-start.1
  6.5 112.8 %all-gather.4.cloned.1.call-start = ((), (), s32[]{:S(2)}) async-start(), calls=%async_computation | async-start | bytes 7208960 | tf_op jit(solution)/shard_map/all_gather | solution.py:35
  9.8 216.1 %all-gather.6.cloned.1.call-start = ((), (), s32[]{:S(2)}) async-start(), calls=%async_computation.1 | async-start | bytes 7208960 | tf_op jit(solution)/shard_map/all_gather | solution.py:36
  11.2 3.4 copy-start.2
  11.2 108.2 %copy-start.5 = (f32[1408]{0:T(1024)S(1)}, f32[1408]{0:T(1024)}, u32[]{:S(2)}) copy-start(f32[1408]{0:T(1024)} %param.12) | copy-start | bytes 16900
  11.2 108.2 %copy-start.6 = (f32[2048]{0:T(1024)S(1)}, f32[2048]{0:T(1024)}, u32[]{:S(2)}) copy-start(f32[2048]{0:T(1024)} %param.10) | copy-start | bytes 24580
  11.2 321.3 %all-gather.8.cloned.1.call-start = ((), (), s32[]{:S(2)}) async-start(), calls=%async_computation.2 | async-start | bytes 7208960 | tf_op jit(solution)/shard_map/all_gather | solution.py:41
  14.5 381.1 %all-reduce.2.cloned.1.call-start = ((), (), s32[]{:S(2)}) async-start(), calls=%async_computation.3 | async-start | bytes 4194304 | tf_op jit(solution)/shard_map/psum | solution.py:43
  15.0 317.4 %copy-start.7 = (f32[1408]{0:T(1024)S(1)}, f32[1408]{0:T(1024)}, u32[]{:S(2)}) copy-start(f32[1408]{0:T(1024)} %param.14) | copy-start | bytes 16900
  127.0 268.6 %copy-start.3 = (f32[2048]{0:T(1024)S(1)}, f32[2048]{0:T(1024)}, u32[]{:S(2)}) copy-start(f32[2048]{0:T(1024)} %param.16) | copy-start | bytes 24580
  345.8 52.2 %copy-start.4 = (f32[2048]{0:T(1024)S(1)}, f32[2048]{0:T(1024)}, u32[]{:S(2)}) copy-start(f32[2048]{0:T(1024)} %param.17) | copy-start | bytes 24580
  395.6 2.4 copy-start
Sparse Core Ops, SparseCore 0:
  9.9 109.3 all-gather.3
  120.9 104.9 all-gather.5
  227.5 104.9 all-gather.7
  345.9 49.6 all-reduce.1
where the time goes:
time: 407 us; the launch traced here: 406 us
  waiting for transfers between devices  360 us (88%)
  matrix products  21 us (5%)
  between operations  13.2 us (3%)
  other arithmetic  12.6 us (3%)
    all_gather x1, waiting for transfers between devices, body(): down_full = lax.all_gather(down_low, 'fs', axis=1, tiled=True)  107 us
    all_gather x1, waiting for transfers between devices, body(): lax.all_gather(gate_low, 'fs', axis=0, tiled=True)  104 us
    all_gather x1, waiting for transfers between devices, body(): lax.all_gather(up_low, 'fs', axis=0, tiled=True)  98.9 us
    psum x1, waiting for transfers between devices, body(): lax.psum(partial_value.astype(jnp.bfloat16), 'tp').astype(jnp.float32)  49.8 us
    dot_general x1, matrix products, body(): jnp.dot(hidden, down_full, preferred_element_type=jnp.float32)  13.3 us
  transfers between devices with their start and end apart: 4, of which 4 were waited for; matrix products, arithmetic and copies ran while one was open for 3% of the time, Pallas kernels for 0%

commit v1 on v0

--- a/solution.py
+++ b/solution.py
@@ -2,8 +2,22 @@
 import jax.numpy as jnp
 from jax import lax
 from jax.sharding import PartitionSpec as P
+from jax.lax import axis_index, ppermute, psum
 
 EPS = 1e-06
+
+
+def lay_fields(x_local):
+    sides = psum(1, "fs")
+    arrivals = [(kk, (kk + 1) % sides) for kk in range(sides)]
+    z_new = [None] * sides
+    z_new[sides - 1] = x_local
+    for nth in range(sides - 2, -1, -1):
+        z_new[nth] = ppermute(z_new[nth + 1], "fs", arrivals)
+    mixed_arr = jnp.concatenate(z_new, 1)
+    z = (axis_index("fs") + 1) * x_local.shape[1]
+    b_next = jnp.roll(mixed_arr, z, 1)
+    return b_next
 
 
 def finish(summed, down_scale, post_gain):
@@ -38,7 +52,7 @@
     gate = jnp.dot(normed, gate_full, preferred_element_type=jnp.float32) * gate_scale
     up = jnp.dot(normed, up_full, preferred_element_type=jnp.float32) * up_scale
     hidden = (jax.nn.silu(gate) * up).astype(jnp.bfloat16)
-    down_full = lax.all_gather(down_low, "fs", axis=1, tiled=True)
+    down_full = lay_fields(down_low)
     partial_value = jnp.dot(hidden, down_full, preferred_element_type=jnp.float32)
     summed = lax.psum(partial_value.astype(jnp.bfloat16), "tp").astype(jnp.float32)
     return finish(summed, down_scale, post_gain)

time: 407 us -> 377 us (0.926)
  waiting for transfers between devices: 360 us -> 272 us
  starting transfers between devices: 0.13 us -> 37.3 us
  local copies, waits for them, and re-layouts: 0.04 us -> 14.3 us
  other arithmetic: 12.6 us -> 17.1 us
    ppermute x0 -> x3, waiting for transfers between devices: none -> 174 us  [lay_fields(): z_new[nth] = ppermute(z_new[nth + 1], 'fs', arrivals)]
    all_gather x1 -> x0, waiting for transfers between devices: 107 us -> none  [body(): down_full = lax.all_gather(down_low, 'fs', axis=1, tiled=True)]
    all_gather x1, waiting for transfers between devices: 104 us -> 0.01 us  [body(): lax.all_gather(gate_low, 'fs', axis=0, tiled=True)]
    all_gather x1, waiting for transfers between devices: 98.9 us -> 48 us  [body(): lax.all_gather(up_low, 'fs', axis=0, tiled=True)]
    ppermute x0 -> x3, starting transfers between devices: none -> 37.2 us  [lay_fields(): z_new[nth] = ppermute(z_new[nth + 1], 'fs', arrivals)]
    unnamed x16 -> x24, local copies, waits for them, and re-layouts: 0.04 us -> 14.3 us
  transfers between devices with their start and end apart: 4 -> 6, of which waited for: 4 -> 5; matrix products, arithmetic and copies ran while one was open for 3% -> 8% of each run, Pallas kernels for 0% -> 0%
where the time goes in v1:
time: 377 us; the launch traced here: 376 us
  waiting for transfers between devices  272 us (72%)
  starting transfers between devices  37.3 us (10%)
  matrix products  21.9 us (6%)
  other arithmetic  17.1 us (5%)
  local copies, waits for them, and re-layouts  14.3 us (4%)
  between operations  13.2 us (4%)
    ppermute x3, waiting for transfers between devices, lay_fields(): z_new[nth] = ppermute(z_new[nth + 1], 'fs', arrivals)  174 us
    psum x1, waiting for transfers between devices, body(): lax.psum(partial_value.astype(jnp.bfloat16), 'tp').astype(jnp.float32)  50.5 us
    all_gather x1, waiting for transfers between devices, body(): lax.all_gather(up_low, 'fs', axis=0, tiled=True)  48 us
    ppermute x3, starting transfers between devices, lay_fields(): z_new[nth] = ppermute(z_new[nth + 1], 'fs', arrivals)  37.2 us
    unnamed x24, local copies, waits for them, and re-layouts  14.3 us
    dot_general x1, matrix products, body(): jnp.dot(hidden, down_full, preferred_element_type=jnp.float32)  13.4 us
    dot_general x1, matrix products, body(): jnp.dot(normed, gate_full, preferred_element_type=jnp.float32) * gate_scale  8.48 us
  transfers between devices with their start and end apart: 6, of which 5 were waited for; matrix products, arithmetic and copies ran while one was open for 8% of the time, Pallas kernels for 0%

profile of v1, /device:TPU:0, one launch (start us, length us, event | category | flops | bytes accessed | tf_op | source)
XLA Modules:
  0.0 376.2 jit_solution(9358879853296601155)
XLA Ops:
  6.5 3.1 convert_element_type.29
  9.6 0.0 all-gather.3.cloned.1.call-update
  9.6 0.0 all-gather.5.cloned.1.call-start
  9.7 3.2 convert_element_type.30
  12.9 0.0 all-gather.5.cloned.1.call-update
  12.9 0.0 all-reduce.2.cloned.1.call-start
  13.0 0.2 convert_element_type.32
  13.2 3.1 collective-permute-start
  16.3 58.6 %collective-permute-done = bf16[1408,512]{1,0:T(8,128)(2,1)S(1)} collective-permute-done((bf16[1408,512]{1,0:T(8,128)(2,1)S(1)}, bf16[1408,512]{1,0:T(8,128)(2,1)S(1)}, u32[]{:S(2)}, u32[]{:S(2)}) %collective-permute-start) | collective-permute-done | bytes 1441824 | tf_op jit(solution)/shard_map/ppermute | solution.py:16
  74.9 1.1 copy-done.1
  76.0 27.7 %collective-permute-start.1 = (bf16[1408,512]{1,0:T(8,128)(2,1)S(1)}, bf16[1408,512]{1,0:T(8,128)(2,1)}, u32[]{:S(2)}, u32[]{:S(2)}) collective-permute-start(bf16[1408,512]{1,0:T(8,128)(2,1)S(1)} %collective-permute-done), channel_id=1, source_target_pairs={{0,4},{4,8},{8,12},{12,0},{1,5},{5,9},{9,13},{13,1},{2,6},{6,10},{... | collective-permute-start | bytes 4325384 | tf_op jit(solution)/shard_map/ppermute | solution.py:16
  103.8 62.1 %collective-permute-done.1 = bf16[1408,512]{1,0:T(8,128)(2,1)} collective-permute-done((bf16[1408,512]{1,0:T(8,128)(2,1)S(1)}, bf16[1408,512]{1,0:T(8,128)(2,1)}, u32[]{:S(2)}, u32[]{:S(2)}) %collective-permute-start.1) | collective-permute-done | bytes 1441824 | tf_op jit(solution)/shard_map/ppermute | solution.py:16
  165.9 6.4 %collective-permute-start.2 = (bf16[1408,512]{1,0:T(8,128)(2,1)}, bf16[1408,512]{1,0:T(8,128)(2,1)}, u32[]{:S(2)}, u32[]{:S(2)}) collective-permute-start(bf16[1408,512]{1,0:T(8,128)(2,1)} %collective-permute-done.1), channel_id=1, source_target_pairs={{0,4},{4,8},{8,12},{12,0},{1,5},{5,9},{9,13},{13,1},{2,6},{6,10},{... | collective-permute-start | bytes 4325384 | tf_op jit(solution)/shard_map/ppermute | solution.py:16
  172.3 2.2 fusion.2
  174.5 53.1 %collective-permute-done.2 = bf16[1408,512]{1,0:T(8,128)(2,1)} collective-permute-done((bf16[1408,512]{1,0:T(8,128)(2,1)}, bf16[1408,512]{1,0:T(8,128)(2,1)}, u32[]{:S(2)}, u32[]{:S(2)}) %collective-permute-start.2) | collective-permute-done | bytes 1441824 | tf_op jit(solution)/shard_map/ppermute | solution.py:16
  227.6 2.6 constant_dynamic-update-slice_fusion.7
  230.1 2.6 constant_dynamic-update-slice_fusion.6
  232.8 1.3 constant_dynamic-update-slice_fusion.5
  234.1 1.3 constant_dynamic-update-slice_fusion.4
  235.4 2.7 constant_dynamic-update-slice_fusion.3
  238.1 2.7 constant_dynamic-update-slice_fusion.2
  240.8 1.3 constant_dynamic-update-slice_fusion.1
  242.1 1.4 constant_dynamic-update-slice_fusion
  243.5 8.5 %convolution_multiply_fusion.1 = f32[512,1408]{1,0:T(8,128)} fusion(bf16[2048,1408]{1,0:T(8,128)(2,1)} %all-gather.3.cloned.1.call-done, f32[1408]{0:T(1024)S(1)} %copy-done.6, bf16[512,2048]{1,0:T(8,128)(2,1)} %param.9, f32[2048]{0:T(1024)S(1)} %copy-done.7, f32[512]{0:T(512)S(1)} %add_rsqrt_fusion.1), kind=kOutput, calls=%fused_computation.12 | convolution fusion | flops 2957705216 | bytes 10763776 | tf_op jit(solution)/shard_map/dot_general | solution.py:52
  251.9 48.0 %all-gather.5.cloned.1.call-done = bf16[2048,1408]{1,0:T(8,128)(2,1)} async-done(((bf16[512,1408]{1,0:T(8,128)(2,1)}), bf16[2048,1408]{1,0:T(8,128)(2,1)}) %all-gather.5.cloned.1.call-update) | async-done | bytes 5767184 | tf_op jit(solution)/shard_map/all_gather | solution.py:50
  300.0 0.0 copy-done.3
  300.0 13.4 %fusion.7 = bf16[512,2048]{1,0:T(8,128)(2,1)} fusion(bf16[1408,4096]{1,0:T(8,128)(2,1)} %constant_dynamic-update-slice_fusion, s32[]{:T(128)S(6)} %select_n.14, bf16[2048,1408]{1,0:T(8,128)(2,1)} %all-gather.5.cloned.1.call-done, f32[512,1408]{1,0:T(8,128)} %convolution_multiply_fusion.1, f32[1408]{0:T(1024)S(1)} %copy-done.8, ...), kind=kOutput, calls=%fused_computation.14 | convolution fusion | flops 5915869184 | bytes 18628100 | tf_op jit(solution)/shard_map/dot_general | solution.py:56
  313.4 0.0 all-reduce.2.cloned.1.call-update
  313.4 50.5 %all-reduce.2.cloned.1.call-done = bf16[512,2048]{1,0:T(8,128)(2,1)} async-done(((bf16[512,2048]{1,0:T(8,128)(2,1)}), bf16[512,2048]{1,0:T(8,128)(2,1)}) %all-reduce.2.cloned.1.call-update) | async-done | bytes 2097168 | tf_op jit(solution)/shard_map/psum | solution.py:57
  363.9 0.0 copy-done.4
  363.9 2.2 multiply_reduce_fusion
  366.1 3.6 multiply_convert_fusion
  (19 shorter events, 0.0 us)
Async XLA Ops:
  6.5 236.9 %all-gather.3.cloned.1.call-start = ((), (), s32[]{:S(2)}) async-start(), calls=%async_computation | async-start | bytes 7208960 | tf_op jit(solution)/shard_map/all_gather | solution.py:49
  9.6 3.4 copy-start
  9.6 290.3 %all-gather.5.cloned.1.call-start = ((), (), s32[]{:S(2)}) async-start(), calls=%async_computation.1 | async-start | bytes 7208960 | tf_op jit(solution)/shard_map/all_gather | solution.py:50
  12.9 351.0 %all-reduce.2.cloned.1.call-start = ((), (), s32[]{:S(2)}) async-start(), calls=%async_computation.2 | async-start | bytes 4194304 | tf_op jit(solution)/shard_map/psum | solution.py:57
  13.2 61.8 %collective-permute-start = (bf16[1408,512]{1,0:T(8,128)(2,1)S(1)}, bf16[1408,512]{1,0:T(8,128)(2,1)S(1)}, u32[]{:S(2)}, u32[]{:S(2)}) collective-permute-start(bf16[1408,512]{1,0:T(8,128)(2,1)S(1)} %convert_element_type.32), channel_id=1, source_target_pairs={{0,4},{4,8},{8,12},{12,0},{1,5},{5,9},{9,13},{13,1},{2,6},{6,10},{... | collective-permute-start | bytes 4325384 | tf_op jit(solution)/shard_map/ppermute | solution.py:16
  74.9 1.1 copy-start.1
  76.0 89.9 %collective-permute-start.1 = (bf16[1408,512]{1,0:T(8,128)(2,1)S(1)}, bf16[1408,512]{1,0:T(8,128)(2,1)}, u32[]{:S(2)}, u32[]{:S(2)}) collective-permute-start(bf16[1408,512]{1,0:T(8,128)(2,1)S(1)} %collective-permute-done), channel_id=1, source_target_pairs={{0,4},{4,8},{8,12},{12,0},{1,5},{5,9},{9,13},{13,1},{2,6},{6,10},{... | collective-permute-start | bytes 4325384 | tf_op jit(solution)/shard_map/ppermute | solution.py:16
  165.9 61.6 %collective-permute-start.2 = (bf16[1408,512]{1,0:T(8,128)(2,1)}, bf16[1408,512]{1,0:T(8,128)(2,1)}, u32[]{:S(2)}, u32[]{:S(2)}) collective-permute-start(bf16[1408,512]{1,0:T(8,128)(2,1)} %collective-permute-done.1), channel_id=1, source_target_pairs={{0,4},{4,8},{8,12},{12,0},{1,5},{5,9},{9,13},{13,1},{2,6},{6,10},{... | collective-permute-start | bytes 4325384 | tf_op jit(solution)/shard_map/ppermute | solution.py:16
  172.3 60.5 %copy-start.2 = (bf16[1408,512]{1,0:T(8,128)(2,1)S(1)}, bf16[1408,512]{1,0:T(8,128)(2,1)}, u32[]{:S(2)}) copy-start(bf16[1408,512]{1,0:T(8,128)(2,1)} %copy-done.1) | copy-start | bytes 4325380
  240.8 2.7 copy-start.6
  240.8 2.7 copy-start.7
  243.4 56.5 %copy-start.3 = (bf16[512,2048]{1,0:T(8,128)(2,1)S(1)}, bf16[512,2048]{1,0:T(8,128)(2,1)}, u32[]{:S(2)}) copy-start(bf16[512,2048]{1,0:T(8,128)(2,1)} %param.9) | copy-start | bytes 6291460
  243.4 56.5 %copy-start.8 = (f32[1408]{0:T(1024)S(1)}, f32[1408]{0:T(1024)}, u32[]{:S(2)}) copy-start(f32[1408]{0:T(1024)} %param.14) | copy-start | bytes 16900
  251.9 112.0 %copy-start.4 = (f32[2048]{0:T(1024)S(1)}, f32[2048]{0:T(1024)}, u32[]{:S(2)}) copy-start(f32[2048]{0:T(1024)} %param.16) | copy-start | bytes 24580
  313.4 52.8 %copy-start.5 = (f32[2048]{0:T(1024)S(1)}, f32[2048]{0:T(1024)}, u32[]{:S(2)}) copy-start(f32[2048]{0:T(1024)} %param.17) | copy-start | bytes 24580
Sparse Core Ops, SparseCore 0:
  9.7 164.2 all-gather.2
  175.6 124.2 all-gather.4
  313.5 50.3 all-reduce.1
